TPU v7x, 32 devices: a whole 2x2x4 slice. The times are simulated.
32 devices in a mesh: sp: 8 (over z, y), tp: 4 (over x, core).
Axes of the slice: x: 2, y: 2, z: 4, core: 2. Of those that a mesh axis runs over, the one named last changes fastest.
Arguments:
- resid_in: bfloat16 [2048, 2048], P('sp'), may hold values from -6 to 6
- query_latent: bfloat16 [2048, 768], P('sp'), may hold values from -6 to 6
- kv_latent: bfloat16 [2048, 512], P('sp'), may hold values from -6 to 6
- rotary_key: bfloat16 [2048, 64], P('sp'), may hold values from -200 to 200
- query_gain: float32 [768], replicated, may hold values from 0.1 to 1.9
- kv_gain: float32 [512], replicated, may hold values from 0.1 to 1.9
- w_query_plain: bfloat16 [768, 2048], P(None, 'tp'), may hold values from -0.875 to 0.875
- w_query_rotary: bfloat16 [768, 1024], P(None, 'tp'), may hold values from -0.875 to 0.875
- w_key_plain: bfloat16 [512, 2048], P(None, 'tp'), may hold values from -0.25 to 0.25
- w_value: bfloat16 [512, 2048], P(None, 'tp'), may hold values from -0.25 to 0.25
- w_output: bfloat16 [2048, 2048], P('tp'), may hold values from -0.125 to 0.125
- ffn_gain: float32 [2048], replicated, may hold values from 0.1 to 1.9
- w_gate: bfloat16 [2048, 5632], P('sp', 'tp'), may hold values from -0.125 to 0.125
- w_up: bfloat16 [2048, 5632], P('sp', 'tp'), may hold values from -0.125 to 0.125
- w_down: bfloat16 [5632, 2048], P('tp', 'sp'), may hold values from -0.078125 to 0.078125
Outputs:
- resid_out: bfloat16 [2048, 2048], P(('sp', 'tp'))
All inputs are finite; a program needn't handle non-finite values.
Results may differ from a plain program's by a relative error of at most 0.014.
The roundings to bfloat16 on the way count: a program that leaves them out, or rounds other values in their place, can miss the bound.
Values may be sent and summed in bfloat16 or wider, within the bound.
No kernel may reach another device: no remote copies, remote signals or barrier semaphores. Data moves between devices by JAX's collectives and lax.ppermute only.
A program may use at most 192 MiB of HBM per device.

v0:
```python
import jax
import jax.numpy as jnp
from jax import lax
from jax.sharding import PartitionSpec as P

NOPE = 128
ROPE = 64
VDIM = 128


def normed(values, gain):
    wide = values.astype(jnp.float32)
    return wide * lax.rsqrt(jnp.mean(wide * wide, axis=-1, keepdims=True) + 1e-06) * gain


def rotate(values, cosine, sine):
    half = values.shape[-1] // 2
    first = values[..., :half]
    second = values[..., half:]
    return jnp.concatenate(
        [first * cosine - second * sine, second * cosine + first * sine], axis=-1
    )


def attend(carry, q_plain, q_rot, k_plain, values, key_rot):
    top, total, acc = carry
    scale = (NOPE + ROPE) ** (-0.5)
    score = (
        jnp.einsum("qhd,khd->hqk", q_plain, k_plain, preferred_element_type=jnp.float32)
        + jnp.einsum("qhr,kr->hqk", q_rot, key_rot, preferred_element_type=jnp.float32)
    ) * scale
    new_top = jnp.maximum(top, jnp.max(score, axis=-1))
    weight = jnp.exp(score - new_top[:, :, None])
    total = jnp.sum(weight, axis=-1)
    mixed = jnp.einsum(
        "hqk,khd->qhd", weight.astype(jnp.bfloat16), values, preferred_element_type=jnp.float32
    )
    acc = mixed
    return (new_top, total, acc)


def shards(
    resid_in,
    query_latent,
    kv_latent,
    rotary_key,
    query_gain,
    kv_gain,
    w_query_plain,
    w_query_rotary,
    w_key_plain,
    w_value,
    w_output,
    ffn_gain,
    w_gate,
    w_up,
    w_down,
):
    tok = resid_in.shape[0]
    heads_dev = w_query_plain.shape[1] // NOPE
    offset = lax.axis_index("sp") * tok
    position = (offset + jnp.arange(tok, dtype=jnp.int32)).astype(jnp.float32)
    freq = 10000.0 ** (-jnp.arange(0, ROPE, 2, dtype=jnp.float32) / ROPE)
    angle = position[:, None] * freq[None, :]
    cosine = jnp.cos(angle)
    sine = jnp.sin(angle)
    q_norm = normed(query_latent, query_gain).astype(jnp.bfloat16)
    kv_norm = normed(kv_latent, kv_gain).astype(jnp.bfloat16)
    key_rot = rotate(rotary_key.astype(jnp.float32), cosine, sine).astype(jnp.bfloat16)
    q_plain = (
        jnp.dot(q_norm, w_query_plain, preferred_element_type=jnp.float32)
        .astype(jnp.bfloat16)
        .reshape(tok, heads_dev, NOPE)
    )
    q_raw = jnp.dot(q_norm, w_query_rotary, preferred_element_type=jnp.float32).reshape(
        tok, heads_dev, ROPE
    )
    q_rot = rotate(q_raw, cosine[:, None, :], sine[:, None, :]).astype(jnp.bfloat16)
    start_carry = (
        jnp.full((heads_dev, tok), -1e30, jnp.float32),
        jnp.zeros((heads_dev, tok), jnp.float32),
        jnp.zeros((tok, heads_dev, VDIM), jnp.float32),
    )
    latent = lax.all_gather(kv_norm, "sp", axis=0, tiled=True)
    rot_piece = lax.all_gather(key_rot, "sp", axis=0, tiled=True)
    count = latent.shape[0]
    k_piece = (
        jnp.dot(latent, w_key_plain, preferred_element_type=jnp.float32)
        .astype(jnp.bfloat16)
        .reshape(count, heads_dev, NOPE)
    )
    v_piece = (
        jnp.dot(latent, w_value, preferred_element_type=jnp.float32)
        .astype(jnp.bfloat16)
        .reshape(count, heads_dev, VDIM)
    )
    top, total, acc = attend(start_carry, q_plain, q_rot, k_piece, v_piece, rot_piece)
    attn = (
        (acc / jnp.transpose(total)[:, :, None]).astype(jnp.bfloat16).reshape(tok, heads_dev * VDIM)
    )
    partial_out = jnp.dot(attn, w_output, preferred_element_type=jnp.float32)
    share = tok // lax.axis_size("tp")
    own_start = lax.axis_index("tp") * share
    mid = resid_in.astype(jnp.float32) + lax.psum(partial_out.astype(jnp.bfloat16), "tp").astype(
        jnp.float32
    )
    h_norm = normed(mid, ffn_gain).astype(jnp.bfloat16)
    mid_own = lax.dynamic_slice_in_dim(mid, own_start, share, 0)
    gate = jnp.dot(
        h_norm, lax.all_gather(w_gate, "sp", axis=0, tiled=True), preferred_element_type=jnp.float32
    )
    upper = jnp.dot(
        h_norm, lax.all_gather(w_up, "sp", axis=0, tiled=True), preferred_element_type=jnp.float32
    )
    hidden = (jax.nn.silu(gate) * upper).astype(jnp.bfloat16)
    terms = jnp.dot(
        hidden, lax.all_gather(w_down, "sp", axis=1, tiled=True), preferred_element_type=jnp.float32
    )
    ffn_own = lax.psum_scatter(
        terms.astype(jnp.bfloat16), "tp", scatter_dimension=0, tiled=True
    ).astype(jnp.float32)
    return (mid_own + ffn_own).astype(jnp.bfloat16)


def solution(mesh):
    return jax.shard_map(
        shards,
        mesh=mesh,
        in_specs=(
            P("sp", None),
            P("sp", None),
            P("sp", None),
            P("sp", None),
            P(),
            P(),
            P(None, "tp"),
            P(None, "tp"),
            P(None, "tp"),
            P(None, "tp"),
            P("tp", None),
            P(),
            P("sp", "tp"),
            P("sp", "tp"),
            P("tp", "sp"),
        ),
        out_specs=P(("sp", "tp"), None),
        check_vma=False,
    )
```

profile of v0, /device:TPU:0, one launch (start us, length us, event | category | flops | bytes accessed | tf_op | source)
XLA Modules:
  0.0 431.7 jit_solution(17128498357206020806)
XLA Ops:
  6.5 1.2 fusion.20
  7.8 1.8 fusion.22
  9.6 0.0 all-reduce.2.cloned.1.call-start
  9.7 0.8 convert_element_type.71
  10.5 0.2 multiply_cosine_fusion
  10.7 32.9 %all_gather.16 = bf16[2048,64]{0,1:T(8,128)(2,1)S(1)} all-gather(bf16[256,64]{0,1:T(8,128)(2,1)S(1)} %pad_maximum_fusion), channel_id=1, replica_groups=mesh['sp'=8,'tp'=4] {'sp'}, dimensions={0}, use_global_device_ids=true | all-gather | bytes 294912 | tf_op jit(solution)/shard_map/all_gather | solution.py:85
  43.6 1.2 fusion.17
  44.8 1.6 fusion.10
  46.4 0.4 fusion.30
  46.9 15.4 %all-gather.5.cloned.1.call-done = bf16[2048,512]{1,0:T(8,128)(2,1)} async-done(((bf16[256,512]{1,0:T(8,128)(2,1)}), bf16[2048,512]{1,0:T(8,128)(2,1)}) %all-gather.5.cloned.1.call-update) | async-done | bytes 2097168 | tf_op jit(solution)/shard_map/all_gather | solution.py:84
  62.3 2.9 convolution_convert_fusion
  65.2 1.2 fusion.23
  66.4 1.4 fusion.36
  67.9 1.3 fusion.1
  69.2 0.3 copy-done.3
  69.4 0.1 copy-done.5
  69.5 1.3 convolution_convert_fusion.1
  70.9 1.8 fusion.14
  72.6 1.7 convolution_convert_fusion.2
  74.4 0.7 all-gather.7.cloned.1.call-update
  75.2 0.5 all-gather.11.cloned.1.call-update
  75.8 0.5 all-gather.9.cloned.1.call-update
  76.3 0.2 reduce-scatter.2.cloned.1.call-start
  76.5 32.9 %all-reduce.2.cloned.1.call-done = bf16[256,2048]{1,0:T(8,128)(2,1)} async-done(((bf16[256,2048]{1,0:T(8,128)(2,1)}), bf16[256,2048]{1,0:T(8,128)(2,1)}) %all-reduce.2.cloned.1.call-update) | async-done | bytes 1048592 | tf_op jit(solution)/shard_map/psum | solution.py:104
  109.4 2.9 convert_add_fusion
  112.4 92.1 %all-gather.7.cloned.1.call-done = bf16[2048,1408]{1,0:T(8,128)(2,1)} async-done(((bf16[256,1408]{1,0:T(8,128)(2,1)}), bf16[2048,1408]{1,0:T(8,128)(2,1)}) %all-gather.7.cloned.1.call-update) | async-done | bytes 5767184 | tf_op jit(solution)/shard_map/all_gather | solution.py:110
  204.5 5.9 %fusion.35 = f32[256,1408]{1,0:T(8,128)} fusion(bf16[2048,1408]{1,0:T(8,128)(2,1)} %all-gather.7.cloned.1.call-done, f32[2048]{0:T(1024)S(1)} %copy-done.7, f32[256]{0:T(256)S(1)} %add_rsqrt_fusion, bf16[256,2048]{1,0:T(8,128)(2,1)} %all-reduce.2.cloned.1.call-done, bf16[256,2048]{1,0:T(8,128)(2,1)S(1)} %copy-done.1), kind=kOutput, calls=%fused_computation.55 | convolution fusion | flops 1479540736 | bytes 9315328 | tf_op jit(solution)/shard_map/dot_general | solution.py:109
  210.4 87.3 %all-gather.11.cloned.1.call-done = bf16[1408,2048]{1,0:T(8,128)(2,1)} async-done(((bf16[1408,256]{1,0:T(8,128)(2,1)}), bf16[1408,2048]{1,0:T(8,128)(2,1)}) %all-gather.11.cloned.1.call-update) | async-done | bytes 5767184 | tf_op jit(solution)/shard_map/all_gather | solution.py:117
  297.7 92.6 %all-gather.9.cloned.1.call-done = bf16[2048,1408]{1,0:T(8,128)(2,1)} async-done(((bf16[256,1408]{1,0:T(8,128)(2,1)}), bf16[2048,1408]{1,0:T(8,128)(2,1)}) %all-gather.9.cloned.1.call-update) | async-done | bytes 5767184 | tf_op jit(solution)/shard_map/all_gather | solution.py:113
  390.2 9.6 %convolution_convert_fusion.3 = bf16[256,2048]{1,0:T(8,128)(2,1)} fusion(bf16[1408,2048]{1,0:T(8,128)(2,1)} %all-gather.11.cloned.1.call-done, bf16[2048,1408]{1,0:T(8,128)(2,1)} %all-gather.9.cloned.1.call-done, f32[256,1408]{1,0:T(8,128)} %fusion.35, f32[2048]{0:T(1024)S(1)} %copy-done.7, f32[256]{0:T(256)S(1)} %add_rsqrt_fusion, ...), kind=kOutput, calls=%fused_computation.12 | convolution fusion | flops 2958622720 | bytes 16131072 | tf_op jit(solution)/shard_map/dot_general | solution.py:116
  399.9 23.1 %reduce-scatter.2.cloned.1.call-done = bf16[64,2048]{1,0:T(8,128)(2,1)} async-done(((bf16[256,2048]{1,0:T(8,128)(2,1)}), bf16[64,2048]{1,0:T(8,128)(2,1)}) %reduce-scatter.2.cloned.1.call-update) | async-done | bytes 262160 | tf_op jit(solution)/shard_map/reduce_scatter | solution.py:119
  423.0 1.9 add_convert_fusion
  (31 shorter events, 0.3 us)
Async XLA Ops:
  6.5 66.1 %copy-start = (bf16[512,2048]{1,0:T(8,128)(2,1)S(1)}, bf16[512,2048]{1,0:T(8,128)(2,1)}, u32[]{:S(2)}) copy-start(bf16[512,2048]{1,0:T(8,128)(2,1)} %param.25) | copy-start | bytes 6291460
  6.5 38.3 %copy-start.2 = (bf16[256,768]{1,0:T(8,128)(2,1)S(1)}, bf16[256,768]{1,0:T(8,128)(2,1)}, u32[]{:S(2)}) copy-start(bf16[256,768]{1,0:T(8,128)(2,1)} %param.16) | copy-start | bytes 1179652
  6.5 38.3 %copy-start.8 = (f32[768]{0:T(1024)S(1)}, f32[768]{0:T(1024)}, u32[]{:S(2)}) copy-start(f32[768]{0:T(1024)} %param.19) | copy-start | bytes 9220
  6.5 55.7 %all-gather.5.cloned.1.call-start = ((), (), s32[]{:S(2)}) async-start(), calls=%async_computation.1 | async-start | bytes 2359296 | tf_op jit(solution)/shard_map/all_gather | solution.py:84
  9.6 99.8 %all-reduce.2.cloned.1.call-start = ((), (), s32[]{:S(2)}) async-start(), calls=%async_computation.2 | async-start | bytes 2097152 | tf_op jit(solution)/shard_map/psum | solution.py:104
  9.7 52.6 %copy-start.4 = (bf16[512,512]{1,0:T(8,128)(2,1)S(1)}, bf16[512,512]{1,0:T(8,128)(2,1)}, u32[]{:S(2)}) copy-start(bf16[512,512]{1,0:T(8,128)(2,1)} %param.23) | copy-start | bytes 1572868
  10.5 35.9 %copy-start.6 = (bf16[768,256]{1,0:T(8,128)(2,1)S(1)}, bf16[768,256]{1,0:T(8,128)(2,1)}, u32[]{:S(2)}) copy-start(bf16[768,256]{1,0:T(8,128)(2,1)} %param.22) | copy-start | bytes 1179652
  67.8 1.6 copy-start.3
  67.9 1.7 copy-start.5
  74.4 35.1 %copy-start.1 = (bf16[256,2048]{1,0:T(8,128)(2,1)S(1)}, bf16[256,2048]{1,0:T(8,128)(2,1)}, u32[]{:S(2)}) copy-start(bf16[256,2048]{1,0:T(8,128)(2,1)} %param.15) | copy-start | bytes 3145732
  74.4 130.1 %all-gather.7.cloned.1.call-start = ((), (), s32[]{:S(2)}) async-start(), calls=%async_computation.3 | async-start | bytes 6488064 | tf_op jit(solution)/shard_map/all_gather | solution.py:110
  75.1 222.6 %all-gather.11.cloned.1.call-start = ((), (), s32[]{:S(2)}) async-start(), calls=%async_computation.5 | async-start | bytes 6488064 | tf_op jit(solution)/shard_map/all_gather | solution.py:117
  75.7 314.5 %all-gather.9.cloned.1.call-start = ((), (), s32[]{:S(2)}) async-start(), calls=%async_computation.4 | async-start | bytes 6488064 | tf_op jit(solution)/shard_map/all_gather | solution.py:113
  76.3 128.2 %copy-start.7 = (f32[2048]{0:T(1024)S(1)}, f32[2048]{0:T(1024)}, u32[]{:S(2)}) copy-start(f32[2048]{0:T(1024)} %param.26) | copy-start | bytes 24580
  76.3 346.7 %reduce-scatter.2.cloned.1.call-start = ((), (), s32[]{:S(2)}) async-start(), calls=%async_computation.6 | async-start | bytes 1310720 | tf_op jit(solution)/shard_map/reduce_scatter | solution.py:119
Sparse Core Ops, SparseCore 0:
  9.7 52.4 all-gather.4
  74.5 34.8 all-reduce.1
  111.6 92.7 all-gather.6
  206.3 91.2 all-gather.10
  299.7 90.4 all-gather.8
  400.0 22.9 reduce-scatter.1
where the time goes:
time: 432 us
  waiting for transfers between devices  345 us (80%)
  blocking collectives  32.9 us (8%)
  matrix products  27.9 us (6%)
  between operations  13.6 us (3%)
  other arithmetic  11.4 us (3%)
    all_gather x1, waiting for transfers between devices, shards(): lax.all_gather(w_up, 'sp', axis=0, tiled=True)  92.6 us
    all_gather x1, waiting for transfers between devices, shards(): lax.all_gather(w_gate, 'sp', axis=0, tiled=True)  92.1 us
    all_gather x1, waiting for transfers between devices, shards(): lax.all_gather(w_down, 'sp', axis=1, tiled=True)  87.3 us
    psum x1, waiting for transfers between devices, shards(): lax.psum(partial_out.astype(jnp.bfloat16), 'tp').astype(jnp.float32)  32.9 us
    all_gather x1, blocking collectives, shards(): rot_piece = lax.all_gather(key_rot, 'sp', axis=0, tiled=True)  32.9 us
    reduce_scatter x1, waiting for transfers between devices, shards(): lax.psum_scatter(terms.astype(jnp.bfloat16), 'tp', scatter_dimension=0, t...  23.1 us
    all_gather x1, waiting for transfers between devices, shards(): latent = lax.all_gather(kv_norm, 'sp', axis=0, tiled=True)  15.4 us
    dot_general x1, matrix products, shards(): jnp.dot(hidden, lax.all_gather(w_down, 'sp', axis=1, tiled=True), preferr...  9.6 us
  transfers between devices with their start and end apart: 6, of which 6 were waited for; matrix products, arithmetic and copies ran while one was open for 3% of the time, Pallas kernels for 0%

commit v1 on v0

--- a/solution.py
+++ b/solution.py
@@ -81,8 +81,13 @@
         jnp.zeros((heads_dev, tok), jnp.float32),
         jnp.zeros((tok, heads_dev, VDIM), jnp.float32),
     )
-    latent = lax.all_gather(kv_norm, "sp", axis=0, tiled=True)
-    rot_piece = lax.all_gather(key_rot, "sp", axis=0, tiled=True)
+    latent, rot_piece = jnp.split(
+        lax.all_gather(
+            jnp.concatenate([kv_norm, key_rot], axis=1), axis_name="sp", axis=0, tiled=True
+        ),
+        [kv_norm.shape[1]],
+        1,
+    )
     count = latent.shape[0]
     k_piece = (
         jnp.dot(latent, w_key_plain, preferred_element_type=jnp.float32)

time: 432 us -> 436 us (level)
  waiting for transfers between devices: 345 us -> 382 us
  blocking collectives: 32.9 us -> 0 us
    all_gather x1, waiting for transfers between devices: 15.4 us -> 53.1 us  [shards(): lax.all_gather(jnp.concatenate([kv_norm, key_rot], axis=1), axis_name='sp...]
    all_gather x1 -> x0, blocking collectives: 32.9 us -> none  [shards(): rot_piece = lax.all_gather(key_rot, 'sp', axis=0, tiled=True)]
where the time goes in v1:
time: 436 us
  waiting for transfers between devices  382 us (88%)
  matrix products  28.9 us (7%)
  between operations  13.6 us (3%)
  other arithmetic  9.1 us (2%)
    all_gather x1, waiting for transfers between devices, shards(): lax.all_gather(w_up, 'sp', axis=0, tiled=True)  92.6 us
    all_gather x1, waiting for transfers between devices, shards(): lax.all_gather(w_gate, 'sp', axis=0, tiled=True)  92.1 us
    all_gather x1, waiting for transfers between devices, shards(): lax.all_gather(w_down, 'sp', axis=1, tiled=True)  87.3 us
    all_gather x1, waiting for transfers between devices, shards(): lax.all_gather(jnp.concatenate([kv_norm, key_rot], axis=1), axis_name='sp...  53.1 us
    psum x1, waiting for transfers between devices, shards(): lax.psum(partial_out.astype(jnp.bfloat16), 'tp').astype(jnp.float32)  32.5 us
    reduce_scatter x1, waiting for transfers between devices, shards(): lax.psum_scatter(terms.astype(jnp.bfloat16), 'tp', scatter_dimension=0, t...  23.1 us
    dot_general x1, matrix products, shards(): jnp.dot(hidden, lax.all_gather(w_down, 'sp', axis=1, tiled=True), preferr...  9.61 us
  transfers between devices with their start and end apart: 6, of which 6 were waited for; matrix products, arithmetic and copies ran while one was open for 3% of the time, Pallas kernels for 0%

profile of v1, /device:TPU:0, one launch (start us, length us, event | category | flops | bytes accessed | tf_op | source)
XLA Modules:
  0.0 436.0 jit_solution(15678040587162184473)
XLA Ops:
  6.6 0.9 convert_element_type.66
  7.5 1.1 copy.16
  8.6 0.1 fusion.22
  8.7 0.8 fusion.24
  9.5 0.2 multiply_cosine_fusion
  9.7 0.7 pad_maximum_fusion
  10.5 0.0 all-reduce.2.cloned.1.call-start
  10.6 0.2 fusion.19
  10.7 1.5 fusion.12
  12.3 1.4 fusion.31
  13.7 53.1 %all-gather.5.cloned.1.call-done = bf16[2048,576]{0,1:T(8,128)(2,1)} async-done(((bf16[256,576]{0,1:T(8,128)(2,1)}), bf16[2048,576]{0,1:T(8,128)(2,1)}) %all-gather.5.cloned.1.call-update) | async-done | bytes 2359312 | tf_op jit(solution)/shard_map/all_gather | solution.py:85
  66.9 2.9 convolution_convert_fusion
  69.8 1.2 fusion.25
  71.0 0.4 copy-done.3
  71.4 1.4 fusion.37
  72.9 1.3 fusion.1
  74.2 1.3 convolution_convert_fusion.1
  75.5 1.8 fusion.16
  77.3 1.7 convolution_convert_fusion.2
  79.1 0.7 all-gather.7.cloned.1.call-update
  79.8 0.5 all-gather.11.cloned.1.call-update
  80.4 0.5 all-gather.9.cloned.1.call-update
  81.0 0.2 reduce-scatter.2.cloned.1.call-start
  81.2 32.5 %all-reduce.2.cloned.1.call-done = bf16[256,2048]{1,0:T(8,128)(2,1)} async-done(((bf16[256,2048]{1,0:T(8,128)(2,1)}), bf16[256,2048]{1,0:T(8,128)(2,1)}) %all-reduce.2.cloned.1.call-update) | async-done | bytes 1048592 | tf_op jit(solution)/shard_map/psum | solution.py:109
  113.7 2.9 convert_add_fusion
  116.6 92.1 %all-gather.7.cloned.1.call-done = bf16[2048,1408]{1,0:T(8,128)(2,1)} async-done(((bf16[256,1408]{1,0:T(8,128)(2,1)}), bf16[2048,1408]{1,0:T(8,128)(2,1)}) %all-gather.7.cloned.1.call-update) | async-done | bytes 5767184 | tf_op jit(solution)/shard_map/all_gather | solution.py:115
  208.7 5.9 %fusion.36 = f32[256,1408]{1,0:T(8,128)} fusion(bf16[2048,1408]{1,0:T(8,128)(2,1)} %all-gather.7.cloned.1.call-done, f32[2048]{0:T(1024)S(1)} %copy-done.6, f32[256]{0:T(256)S(1)} %add_rsqrt_fusion, bf16[256,2048]{1,0:T(8,128)(2,1)} %all-reduce.2.cloned.1.call-done, bf16[256,2048]{1,0:T(8,128)(2,1)S(1)} %copy-done.1), kind=kOutput, calls=%fused_computation.57 | convolution fusion | flops 1479540736 | bytes 9315328 | tf_op jit(solution)/shard_map/dot_general | solution.py:114
  214.6 87.3 %all-gather.11.cloned.1.call-done = bf16[1408,2048]{1,0:T(8,128)(2,1)} async-done(((bf16[1408,256]{1,0:T(8,128)(2,1)}), bf16[1408,2048]{1,0:T(8,128)(2,1)}) %all-gather.11.cloned.1.call-update) | async-done | bytes 5767184 | tf_op jit(solution)/shard_map/all_gather | solution.py:122
  301.9 92.6 %all-gather.9.cloned.1.call-done = bf16[2048,1408]{1,0:T(8,128)(2,1)} async-done(((bf16[256,1408]{1,0:T(8,128)(2,1)}), bf16[2048,1408]{1,0:T(8,128)(2,1)}) %all-gather.9.cloned.1.call-update) | async-done | bytes 5767184 | tf_op jit(solution)/shard_map/all_gather | solution.py:118
  394.5 9.6 %convolution_convert_fusion.3 = bf16[256,2048]{1,0:T(8,128)(2,1)} fusion(bf16[1408,2048]{1,0:T(8,128)(2,1)} %all-gather.11.cloned.1.call-done, bf16[2048,1408]{1,0:T(8,128)(2,1)} %all-gather.9.cloned.1.call-done, f32[256,1408]{1,0:T(8,128)} %fusion.36, f32[2048]{0:T(1024)S(1)} %copy-done.6, f32[256]{0:T(256)S(1)} %add_rsqrt_fusion, ...), kind=kOutput, calls=%fused_computation.12 | convolution fusion | flops 2958622720 | bytes 16131072 | tf_op jit(solution)/shard_map/dot_general | solution.py:121
  404.1 23.1 %reduce-scatter.2.cloned.1.call-done = bf16[64,2048]{1,0:T(8,128)(2,1)} async-done(((bf16[256,2048]{1,0:T(8,128)(2,1)}), bf16[64,2048]{1,0:T(8,128)(2,1)}) %reduce-scatter.2.cloned.1.call-update) | async-done | bytes 262160 | tf_op jit(solution)/shard_map/reduce_scatter | solution.py:124
  427.3 1.9 add_convert_fusion
  (29 shorter events, 0.3 us)
Async XLA Ops:
  6.5 70.8 %copy-start = (bf16[512,2048]{1,0:T(8,128)(2,1)S(1)}, bf16[512,2048]{1,0:T(8,128)(2,1)}, u32[]{:S(2)}) copy-start(bf16[512,2048]{1,0:T(8,128)(2,1)} %param.25) | copy-start | bytes 6291460
  6.5 4.0 copy-start.2
  6.5 4.2 copy-start.7
  6.5 60.3 %all-gather.5.cloned.1.call-start = ((), (), s32[]{:S(2)}) async-start(), calls=%async_computation.1 | async-start | bytes 2654208 | tf_op jit(solution)/shard_map/all_gather | solution.py:85
  9.7 57.2 %copy-start.4 = (bf16[512,512]{1,0:T(8,128)(2,1)S(1)}, bf16[512,512]{1,0:T(8,128)(2,1)}, u32[]{:S(2)}) copy-start(bf16[512,512]{1,0:T(8,128)(2,1)} %param.23) | copy-start | bytes 1572868
  10.5 103.2 %all-reduce.2.cloned.1.call-start = ((), (), s32[]{:S(2)}) async-start(), calls=%async_computation.2 | async-start | bytes 2097152 | tf_op jit(solution)/shard_map/psum | solution.py:109
  69.8 1.7 copy-start.3
  72.9 1.3 copy-start.5
  79.0 34.6 %copy-start.1 = (bf16[256,2048]{1,0:T(8,128)(2,1)S(1)}, bf16[256,2048]{1,0:T(8,128)(2,1)}, u32[]{:S(2)}) copy-start(bf16[256,2048]{1,0:T(8,128)(2,1)} %param.15) | copy-start | bytes 3145732
  79.1 129.6 %all-gather.7.cloned.1.call-start = ((), (), s32[]{:S(2)}) async-start(), calls=%async_computation.3 | async-start | bytes 6488064 | tf_op jit(solution)/shard_map/all_gather | solution.py:115
  79.8 222.1 %all-gather.11.cloned.1.call-start = ((), (), s32[]{:S(2)}) async-start(), calls=%async_computation.5 | async-start | bytes 6488064 | tf_op jit(solution)/shard_map/all_gather | solution.py:122
  80.4 314.1 %all-gather.9.cloned.1.call-start = ((), (), s32[]{:S(2)}) async-start(), calls=%async_computation.4 | async-start | bytes 6488064 | tf_op jit(solution)/shard_map/all_gather | solution.py:118
  81.0 127.7 %copy-start.6 = (f32[2048]{0:T(1024)S(1)}, f32[2048]{0:T(1024)}, u32[]{:S(2)}) copy-start(f32[2048]{0:T(1024)} %param.26) | copy-start | bytes 24580
  81.0 346.3 %reduce-scatter.2.cloned.1.call-start = ((), (), s32[]{:S(2)}) async-start(), calls=%async_computation.6 | async-start | bytes 1310720 | tf_op jit(solution)/shard_map/reduce_scatter | solution.py:124
Sparse Core Ops, SparseCore 0:
  10.6 56.2 all-gather.4
  79.2 34.4 all-reduce.1
  115.9 92.7 all-gather.6
  210.6 91.3 all-gather.10
  304.0 90.4 all-gather.8
  404.2 22.9 reduce-scatter.1
